TPU v7x, 32 devices: a whole 2x2x4 slice. The times are simulated.
32 devices in a mesh: ep: 8 (over z, y), tp: 4 (over x, core).
Axes of the slice: x: 2, y: 2, z: 4, core: 2. Of those that a mesh axis runs over, the one named last changes fastest.
Arguments:
- tokens: bfloat16 [1024, 2048], P('ep'), may hold values from -6 to 6
- out_grad: bfloat16 [1024, 2048], P('ep'), may hold values from -50 to 50
- expert_ids: int32 [1024, 2], P('ep'), may hold values from 0 to 7, all different within a row; in each aligned block of 128 rows (0 to 127, 128 to 255, ...) at most 40 rows name the same one
- route_weights: float32 [1024, 2], P('ep'), may hold values from 0.2 to 2
- gate_proj: bfloat16 [8, 2048, 2048], P('ep', 'tp'), may hold values from -0.125 to 0.125
- up_proj: bfloat16 [8, 2048, 2048], P('ep', 'tp'), may hold values from -0.125 to 0.125
- down_proj: bfloat16 [8, 2048, 2048], P('ep', 'tp'), may hold values from -0.125 to 0.125
- shared_act: bfloat16 [1024, 1024], P('ep'), may hold values from -0.29882812 to 0.29882812
Outputs:
- token_grad: bfloat16 [1024, 2048], P('ep', 'tp')
- route_grad: float32 [1024, 2], P('ep')
- gate_grad: bfloat16 [8, 2048, 2048], P('ep', 'tp')
- up_grad: bfloat16 [8, 2048, 2048], P('ep', 'tp')
- down_grad: bfloat16 [8, 2048, 2048], P('ep', 'tp')
- row_norms: float32 [8, 3, 2048], P('ep', None, 'tp')
- shared_grad: float32 [1024, 2048], P('tp', 'ep')
- shared_norms: float32 [1024], P('tp')
Inputs may be any that keep to these rules, and one draw needn't show every extreme that they name: `expert_ids`: each row names 2 different experts. In the rows of one device no expert is named more than 40 times, and in some device some expert is named exactly 40 times.
All inputs are finite; a program needn't handle non-finite values.
Results may differ from a plain program's by a relative error of at most 0.008.
Values may be sent and summed in bfloat16 or wider, within the bound.
A program may use at most 64 MiB of HBM per device.

v0:
```python
import functools

import jax
import jax.numpy as jnp
from jax import lax
from jax.experimental import pallas as pl
from jax.experimental.pallas import tpu as pltpu
from jax.sharding import PartitionSpec as P


def plain(tokens, out_grad, expert_ids, route_weights, gate_proj, up_proj, down_proj, shared_act):
    ep_count = lax.axis_size("ep")
    tp_count = lax.axis_size("tp")
    tok_count, model_width = tokens.shape
    top_count = expert_ids.shape[1]
    exp_local = gate_proj.shape[0]
    experts = exp_local * ep_count
    capacity = 5 * tok_count * top_count // (4 * experts)
    slot_count = experts * capacity
    assign = tok_count * top_count
    columns = model_width // tp_count
    offset = lax.axis_index("tp") * columns
    flat_expert = expert_ids.reshape(assign)
    onehot = (flat_expert[:, None] == jnp.arange(experts, dtype=jnp.int32)[None, :]).astype(
        jnp.float32
    )
    earlier = (jnp.arange(assign)[:, None] > jnp.arange(assign)[None, :]).astype(jnp.float32)
    counted = jnp.dot(earlier, onehot, precision=lax.Precision.HIGHEST)
    rank_in = jnp.sum(counted * onehot, 1).astype(jnp.int32)
    slot_id = flat_expert * capacity + rank_in
    picked = (jnp.arange(slot_count, dtype=jnp.int32)[:, None] == slot_id[None, :]).astype(
        jnp.float32
    )
    source_id = jnp.dot(
        picked, jnp.arange(assign, dtype=jnp.float32), precision=lax.Precision.HIGHEST
    ).astype(jnp.int32)
    filled = jnp.sum(picked, 1) > 0.5
    scaled = (
        (route_weights[:, :, None] * out_grad[:, None, :])
        .astype(jnp.bfloat16)
        .reshape(assign, model_width)
    )

    def slot_rows(source_rows, row_index):
        taken = jnp.take(source_rows, row_index, axis=0)
        return jnp.where(filled[:, None], taken, jnp.zeros((), source_rows.dtype))

    token_part = lax.dynamic_slice_in_dim(tokens, offset, columns, 1)
    scaled_part = lax.dynamic_slice_in_dim(scaled, offset, columns, 1)
    send_in = slot_rows(token_part, source_id // top_count).reshape(
        ep_count, exp_local, capacity, columns
    )
    send_cot = slot_rows(scaled_part, source_id).reshape(ep_count, exp_local, capacity, columns)
    part_in, part_cot = (
        lax.all_to_all(send_in, "ep", split_axis=0, concat_axis=2, tiled=True),
        lax.all_to_all(send_cot, "ep", split_axis=0, concat_axis=2, tiled=True),
    )
    joined_in, joined_cot = (
        lax.all_gather(part_in, "tp", axis=3, tiled=True),
        lax.all_gather(part_cot, "tp", axis=3, tiled=True),
    )
    rows_in = joined_in[0]
    rows_cot = joined_cot[0]
    gate_pre = jnp.einsum("erd,efd->erf", rows_in, gate_proj, preferred_element_type=jnp.float32)
    up_pre = jnp.einsum("erd,efd->erf", rows_in, up_proj, preferred_element_type=jnp.float32)
    sigmoid_a = jax.nn.sigmoid(gate_pre)
    silu_a = gate_pre * sigmoid_a
    hidden = (silu_a * up_pre).astype(jnp.bfloat16)
    hidden_grad = jnp.einsum(
        "erd,efd->erf", rows_cot, down_proj, preferred_element_type=jnp.float32
    )
    up_delta = (hidden_grad * silu_a).astype(jnp.bfloat16)
    gate_delta = (hidden_grad * up_pre * sigmoid_a * (1.0 + gate_pre * (1.0 - sigmoid_a))).astype(
        jnp.bfloat16
    )
    gate_full = jnp.einsum("erf,erd->efd", gate_delta, rows_in, preferred_element_type=jnp.float32)
    up_full = jnp.einsum("erf,erd->efd", up_delta, rows_in, preferred_element_type=jnp.float32)
    down_full = jnp.einsum("erf,erd->efd", hidden, rows_cot, preferred_element_type=jnp.float32)
    row_norms = jnp.stack(
        [
            jnp.sum(gate_full * gate_full, 2),
            jnp.sum(up_full * up_full, 2),
            jnp.sum(down_full * down_full, 2),
        ],
        axis=1,
    )
    row_total = rows_in.shape[1]
    partial_value = jnp.einsum(
        "erf,efd->erd", gate_delta, gate_proj, preferred_element_type=jnp.float32
    )
    partial_value = partial_value + jnp.einsum(
        "erf,efd->erd", up_delta, up_proj, preferred_element_type=jnp.float32
    )
    partials = partial_value.astype(jnp.bfloat16).reshape(exp_local, row_total, tp_count, columns)
    inner_part = jnp.sum(hidden.astype(jnp.float32) * hidden_grad, 2).astype(jnp.bfloat16)
    inner_parts = jnp.broadcast_to(inner_part[:, :, None], (exp_local, row_total, tp_count))
    received, received_inner = (
        lax.all_to_all(partials, "tp", split_axis=2, concat_axis=2, tiled=True),
        lax.all_to_all(inner_parts, "tp", split_axis=2, concat_axis=2, tiled=True),
    )
    slot_grad = jnp.sum(received.astype(jnp.float32), 2)
    inner = jnp.sum(received_inner.astype(jnp.float32), 2)
    returned, returned_inner = (
        lax.all_to_all(
            slot_grad.reshape(exp_local, ep_count, capacity, columns),
            "ep",
            split_axis=1,
            concat_axis=0,
            tiled=True,
        ),
        lax.all_to_all(
            inner.reshape(exp_local, ep_count, capacity),
            "ep",
            split_axis=1,
            concat_axis=0,
            tiled=True,
        ),
    )
    slot_back = returned.reshape(slot_count, columns)
    inner_back = returned_inner.reshape(slot_count)
    token_grad = jnp.take(slot_back, slot_id, axis=0).reshape(tok_count, top_count, columns).sum(1)
    route_grad = jnp.take(inner_back, slot_id).reshape(tok_count, top_count) / route_weights
    shared_rows = shared_act.shape[1] // tp_count
    shared_part = lax.dynamic_slice_in_dim(
        shared_act, lax.axis_index("tp") * shared_rows, shared_rows, 1
    )
    shared_term = lax.dot_general(
        shared_part, out_grad, (((0,), (0,)), ((), ())), preferred_element_type=jnp.float32
    )
    shared_grad = lax.psum_scatter(shared_term, "ep", scatter_dimension=1, tiled=True)
    shared_norms = lax.psum(jnp.sum(shared_grad * shared_grad, 1), "ep")
    return (
        token_grad.astype(jnp.bfloat16),
        route_grad,
        gate_full.astype(jnp.bfloat16),
        up_full.astype(jnp.bfloat16),
        down_full.astype(jnp.bfloat16),
        row_norms,
        shared_grad,
        shared_norms,
    )


MESH = pl.DeviceIdType.MESH
F32 = jnp.float32
BF16 = jnp.bfloat16
NT = (((1,), (1,)), ((), ()))


def column_to_row(col, width=128):
    return jnp.broadcast_to(col, (col.shape[0], width)).T[0:1]


def kernel(
    n, t, cap, slot,
    ids_ref, rw_ref, tok_hbm, og_hbm, act_hbm, wg_hbm, wu_hbm, wd_hbm,
    token_out, route_out, gate_out, up_out, down_out, norms_out, shared_out, snorm_out,
    send, rows, wg, wu, wd, picks, delta, turned, grads, squares,
    pair_send, pair_recv, acc_far, acc_own, far_send, far_recv, back_send, back_recv,
    inner_tp, inner_tot, inner_ep, act_send, act_all, og_send, og_all, snorm_all,
    tok_part, og_part, og_mine, act_part, l_sem,
    w_sem, g_sem, d_s, d_r, m_s, m_r, c_s, c_r, a_s, a_r, o_s, o_r, q_s, q_r,
    p_s, p_r, f_s, f_r, b_s, b_r, i_s, i_r, j_s, j_r, n_s, n_r,
):
    me = lax.axis_index("ep")
    p = lax.axis_index("tp")
    buddy = p + 1 - 2 * lax.rem(p, 2)
    half = t // 2
    mirror = lax.rem(p + half, t)
    mirror_buddy = lax.rem(buddy + half, t)
    toks, width = tok_hbm.shape
    cols = width // t
    hid = wg.shape[0]
    total = n * slot

    def span(q, size):
        return pl.ds(pl.multiple_of(q * size, 128), size)

    def ahead(i):
        out, bit = 0, 1
        while bit < n:
            digit = lax.rem(me // bit, 2)
            out = out + bit * (1 - digit if i // bit % 2 else digit)
            bit *= 2
        return out

    behind = ahead

    def tp_ahead(i):
        return lax.rem(p + i, t)

    def tp_behind(i):
        return lax.rem(p - i + t, t)

    def copy(src, dst, s_sem, r_sem, where):
        return pltpu.make_async_remote_copy(
            src_ref=src, dst_ref=dst, send_sem=s_sem, recv_sem=r_sem,
            device_id=where, device_id_type=MESH,
        )

    weights = [
        pltpu.make_async_copy(wg_hbm.at[0], wg, w_sem.at[0]),
        pltpu.make_async_copy(wu_hbm.at[0], wu, w_sem.at[1]),
        pltpu.make_async_copy(wd_hbm.at[0], wd, w_sem.at[2]),
    ]
    part = toks // t
    sh = act_hbm.shape[1] // t
    cut = width // n
    loads = [
        pltpu.make_async_copy(tok_hbm.at[:, span(p, cols)], tok_part, l_sem.at[0]),
        pltpu.make_async_copy(og_hbm.at[:, span(p, cols)], og_part, l_sem.at[1]),
        pltpu.make_async_copy(
            og_hbm.at[pl.ds(pl.multiple_of(p * part, 16), part), :], og_mine, l_sem.at[2]
        ),
        pltpu.make_async_copy(act_hbm.at[:, span(p, sh)], act_part, l_sem.at[3]),
    ]
    for load in loads:
        load.start()
    if slot != cap:
        rows[:, :, cap:, :] = jnp.zeros((2, n, slot - cap, width), BF16)
    barrier = pltpu.get_barrier_semaphore()
    for i in range(1, n):
        pl.semaphore_signal(barrier, inc=1, device_id={"ep": ahead(i)}, device_id_type=MESH)
    for i in range(1, t):
        pl.semaphore_signal(barrier, inc=1, device_id={"tp": tp_ahead(i)}, device_id_type=MESH)
    for w in weights:
        w.start()

    expert = lax.broadcasted_iota(jnp.int32, (128, toks), 0)
    first = ids_ref[0:1, :] == expert
    second = ids_ref[1:2, :] == expert
    member = jnp.where(first | second, 1.0, 0.0).astype(F32)
    weight_t = jnp.where(first, rw_ref[0:1, :], jnp.where(second, rw_ref[1:2, :], 0.0))
    upper = lax.broadcasted_iota(jnp.int32, (toks, toks), 0) < lax.broadcasted_iota(
        jnp.int32, (toks, toks), 1
    )
    upper = jnp.where(upper, 1.0, 0.0).astype(BF16)
    rank_t = jnp.dot(member.astype(BF16), upper, preferred_element_type=F32)
    place_t = jnp.where(member > 0.5, rank_t, -1.0)
    row_in = lax.broadcasted_iota(jnp.int32, (slot, toks), 0).astype(F32)
    slot_weight = []
    for e in range(n):
        hit = jnp.where(place_t[e : e + 1] == row_in, 1.0, 0.0).astype(F32)
        picks[e * slot : (e + 1) * slot, :] = hit.astype(BF16)
        slot_weight.append(jnp.sum(hit * weight_t[e : e + 1], 1, keepdims=True))
    slot_weight = jnp.concatenate(slot_weight, 0)
    for load in loads:
        load.wait()
    got = jnp.dot(picks[...], tok_part[...], preferred_element_type=F32).astype(BF16)
    send[:, 0] = got.reshape(n, slot, cols)
    got = jnp.dot(picks[...], og_part[...], preferred_element_type=F32)
    send[:, 1] = (got * slot_weight).astype(BF16).reshape(n, slot, cols)
    for j in range(2):
        rows[j, me, :, span(p, cols)] = send[me, j]
    pl.semaphore_wait(barrier, n + t - 2)

    def chunk(s, q):
        return rows.at[:, s, pl.ds(0, cap), span(q, cols)]

    def dispatch(i):
        return copy(
            send.at[ahead(i), :, pl.ds(0, cap), :], chunk(me, p), d_s.at[i], d_r.at[i],
            {"ep": ahead(i)},
        )

    def to_mirror(i):
        s = behind(i)
        return copy(chunk(s, p), chunk(s, p), m_s.at[i], m_r.at[i], {"tp": mirror})

    def to_buddy(i):
        s = behind(i)
        return copy(chunk(s, p), chunk(s, p), c_s.at[0, i], c_r.at[0, i], {"tp": buddy})

    def on_buddy(i):
        s = behind(i)
        return copy(
            chunk(s, mirror), chunk(s, mirror), c_s.at[1, i], c_r.at[1, i], {"tp": buddy}
        )

    def act_copy(i):
        return copy(act_send, act_all.at[:, me], a_s.at[i], a_r.at[i], {"ep": ahead(i)})

    def og_copy(i):
        return copy(
            og_send.at[ahead(i)], og_all.at[p, me], o_s.at[i], o_r.at[i], {"ep": ahead(i)}
        )

    def og_spread(i):
        return copy(og_all.at[p], og_all.at[p], q_s.at[i], q_r.at[i], {"tp": tp_ahead(i)})

    order = list(range(1, n))
    for i in order:
        dispatch(i).start()
    act_send[...] = act_part[...].reshape(t, part, sh)
    for e in range(n):
        og_send[e] = og_mine[:, e * cut : (e + 1) * cut]
    act_all[:, me] = act_send[...]
    og_all[p, me] = og_send[me]
    for i in range(n):
        if i:
            dispatch(i).wait_recv()
        to_mirror(i).start()
        to_buddy(i).start()
        if i:
            to_mirror(i - 1).wait_recv()
            on_buddy(i - 1).start()
    to_mirror(n - 1).wait_recv()
    on_buddy(n - 1).start()
    for i in order:
        og_copy(i).start()
    for i in order:
        act_copy(i).start()
    for w in weights:
        w.wait()
    for i in range(n):
        to_buddy(i).wait_recv()
        on_buddy(i).wait_recv()

    x_in = rows[0].reshape(total, width)
    x_cot = rows[1].reshape(total, width)
    tile = min(hid, 256)

    def forward(f, inner):
        at = pl.ds(pl.multiple_of(f * tile, tile), tile)
        gate_pre = lax.dot_general(x_in, wg[at, :], NT, preferred_element_type=F32)
        up_pre = lax.dot_general(x_in, wu[at, :], NT, preferred_element_type=F32)
        hidden_grad = lax.dot_general(x_cot, wd[at, :], NT, preferred_element_type=F32)
        sig = jax.nn.sigmoid(gate_pre)
        silu = gate_pre * sig
        hidden = (silu * up_pre).astype(BF16).astype(F32)
        up_d = hidden_grad * silu
        gate_d = hidden_grad * up_pre * sig * (1.0 + gate_pre * (1.0 - sig))
        delta[0, :, at] = gate_d.astype(BF16)
        delta[1, :, at] = up_d.astype(BF16)
        turned[0, at, :] = gate_d.T.astype(BF16)
        turned[1, at, :] = up_d.T.astype(BF16)
        turned[2, at, :] = hidden.T.astype(BF16)
        return inner + jnp.sum(hidden * hidden_grad, 1, keepdims=True)

    inner = lax.fori_loop(0, hid // tile, forward, jnp.zeros((total, 1), F32))
    inner_tp[p] = column_to_row(inner)

    def inner_copy(i):
        return copy(inner_tp.at[p], inner_tp.at[p], i_s.at[i], i_r.at[i], {"tp": tp_ahead(i)})

    for i in range(1, t):
        inner_copy(i).start()

    def share(q):
        at = span(q, cols)
        value = jnp.dot(delta[0], wg[:, at], preferred_element_type=F32)
        return value + jnp.dot(delta[1], wu[:, at], preferred_element_type=F32)

    def pair_copy(k):
        return copy(pair_send.at[k], pair_recv.at[k], p_s.at[k], p_r.at[k], {"tp": buddy})

    pair_send[0] = share(mirror_buddy).astype(BF16)
    pair_copy(0).start()
    acc_far[...] = share(mirror)
    pair_send[1] = share(buddy).astype(BF16)
    pair_copy(1).start()

    def far_copy(i):
        s = behind(i)
        return copy(far_send.at[s], far_recv.at[s], f_s.at[i], f_r.at[i], {"tp": mirror})

    pair_copy(0).wait_recv()
    far = acc_far[...] + pair_recv[0].astype(F32)
    far_send[...] = far.astype(BF16).reshape(n, slot, cols)
    back_order = list(range(1, n)) + [0]
    for i in back_order:
        far_copy(i).start()
    acc_own[...] = share(p).reshape(n, slot, cols)
    pair_copy(1).wait_recv()
    acc_own[...] = acc_own[...] + pair_recv[1].astype(F32).reshape(n, slot, cols)

    for i in range(1, t):
        inner_copy(i).wait_recv()
    inner_tot[...] = jnp.sum(inner_tp[...], 0)
    inner_ep[me] = inner_tot[...]

    def inner_back(i):
        return copy(inner_tot, inner_ep.at[me], j_s.at[i], j_r.at[i], {"ep": ahead(i)})

    for i in range(1, n):
        inner_back(i).start()

    def back_copy(i):
        return copy(
            back_send.at[behind(i), pl.ds(0, cap), :], back_recv.at[me, pl.ds(0, cap), :],
            b_s.at[i], b_r.at[i], {"ep": behind(i)},
        )

    if slot != cap:
        back_recv[:, cap:, :] = jnp.zeros((n, slot - cap, cols), BF16)
    for i in back_order:
        s = behind(i)
        far_copy(i).wait_recv()
        value = (acc_own[s] + far_recv[s].astype(F32)).astype(BF16)
        if i:
            back_send[s] = value
            back_copy(i).start()
        else:
            back_recv[me, 0:cap, :] = value[0:cap]

    for i in range(1, n):
        og_copy(i).wait_recv()
    for i in range(1, t):
        og_spread(i).start()
    for i in range(1, n):
        act_copy(i).wait_recv()

    block = min(width, 256)

    def grad_of(j, source):
        squares[...] = jnp.zeros_like(squares)

        def step(c, carry):
            at = pl.ds(pl.multiple_of(c * block, block), block)
            value = jnp.dot(
                turned[j], rows[source, :, :, at].reshape(total, block),
                preferred_element_type=F32,
            )
            grads[j, :, at] = value.astype(BF16)
            sq = value * value
            here = squares[...]
            for k in range(block // 128):
                here = here + sq[:, k * 128 : (k + 1) * 128]
            squares[...] = here
            return carry

        lax.fori_loop(0, width // block, step, 0)
        norms_out[j] = column_to_row(jnp.sum(squares[...], 1, keepdims=True))

    outs = [
        pltpu.make_async_copy(grads.at[j], out, g_sem.at[j])
        for j, out in enumerate((gate_out, up_out, down_out))
    ]
    grad_of(0, 0)
    outs[0].start()
    for i in range(1, t):
        og_spread(i).wait_recv()
    shared = lax.dot_general(
        act_all[...].reshape(n * toks, sh), og_all[...].reshape(n * toks, cut),
        (((0,), (0,)), ((), ())), preferred_element_type=F32,
    )
    shared_out[...] = shared
    snorm_all[me] = column_to_row(jnp.sum(shared * shared, 1, keepdims=True))

    def snorm_copy(i):
        return copy(
            snorm_all.at[me], snorm_all.at[me], n_s.at[i], n_r.at[i], {"ep": ahead(i)}
        )

    for i in range(1, n):
        snorm_copy(i).start()
    grad_of(1, 0)
    outs[1].start()
    grad_of(2, 1)
    outs[2].start()

    for i in range(1, n):
        inner_back(i).wait_recv()
    at_lane = lax.broadcasted_iota(jnp.int32, (toks, total), 1).astype(F32)
    base = (me * slot).astype(F32)
    rank = place_t.T
    found = jnp.zeros((toks, 128), F32)
    column = lax.broadcasted_iota(jnp.int32, (toks, 128), 1)
    for e in range(n):
        hit = at_lane == (rank[:, e : e + 1] + base)
        value = jnp.sum(jnp.where(hit, inner_ep[e], 0.0), 1, keepdims=True)
        found = jnp.where(column == e, value, found)
    found = found.T
    for k, chosen in enumerate((first, second)):
        value = jnp.sum(jnp.where(chosen, found, 0.0), 0, keepdims=True)
        route_out[k : k + 1, :] = value / rw_ref[k : k + 1, :]
    for i in range(1, n):
        back_copy(i).wait_recv()
    token_out[...] = lax.dot_general(
        picks[...], back_recv[...].reshape(total, cols), (((0,), (0,)), ((), ())),
        preferred_element_type=F32,
    ).astype(BF16)
    for i in range(1, n):
        snorm_copy(i).wait_recv()
    snorm_out[...] = jnp.sum(snorm_all[...], 0)

    for i in range(1, n):
        dispatch(i).wait_send()
        og_copy(i).wait_send()
        act_copy(i).wait_send()
        inner_back(i).wait_send()
        back_copy(i).wait_send()
        snorm_copy(i).wait_send()
    for i in range(n):
        to_mirror(i).wait_send()
        to_buddy(i).wait_send()
        on_buddy(i).wait_send()
        far_copy(i).wait_send()
    for i in range(1, t):
        og_spread(i).wait_send()
        inner_copy(i).wait_send()
    pair_copy(0).wait_send()
    pair_copy(1).wait_send()
    for out in outs:
        out.wait()


def hand_over(*refs):
    count = (len(refs) - 2) // 3
    sources, targets, held = refs[:count], refs[count : 2 * count], refs[2 * count : 3 * count]
    in_sem, out_sem = refs[-2:]
    order = sorted(range(count), key=lambda j: sources[j].size)
    taken, given = [], []
    for j in order:
        top = sources[j].shape[0]
        pieces = 2 if top % 256 == 0 else 1
        for k in range(pieces):
            at = pl.ds(k * (top // pieces), top // pieces)
            sem = 2 * j + k
            taken.append(
                pltpu.make_async_copy(sources[j].at[at], held[j].at[at], in_sem.at[sem])
            )
            given.append(
                pltpu.make_async_copy(held[j].at[at], targets[j].at[at], out_sem.at[sem])
            )
    for move in taken:
        move.start()
    for move, after in zip(taken, given):
        move.wait()
        after.start()
    for after in given:
        after.wait()


def fused(tokens, out_grad, expert_ids, route_weights, gate_proj, up_proj, down_proj, shared_act):
    n = lax.axis_size("ep")
    t = lax.axis_size("tp")
    toks, width = tokens.shape
    experts = gate_proj.shape[0] * n
    cap = 5 * toks * expert_ids.shape[1] // (4 * experts)
    slot = -(-cap // 16) * 16
    hid = gate_proj.shape[1]
    cols = width // t
    sh = shared_act.shape[1] // t
    cut = width // n
    part = toks // t
    total = n * slot
    vmem = pl.BlockSpec(memory_space=pltpu.VMEM)
    hbm = pl.BlockSpec(memory_space=pl.ANY)
    dma = pltpu.SemaphoreType.DMA
    results = pl.pallas_call(
        functools.partial(kernel, n, t, cap, slot),
        out_shape=(
            jax.ShapeDtypeStruct((toks, cols), BF16),
            jax.ShapeDtypeStruct((2, toks), F32),
            jax.ShapeDtypeStruct((hid, width), BF16),
            jax.ShapeDtypeStruct((hid, width), BF16),
            jax.ShapeDtypeStruct((hid, width), BF16),
            jax.ShapeDtypeStruct((3, 1, hid), F32),
            jax.ShapeDtypeStruct((sh, cut), F32),
            jax.ShapeDtypeStruct((1, sh), F32),
        ),
        in_specs=[vmem] * 2 + [hbm] * 6,
        out_specs=(vmem, vmem, hbm, hbm, hbm, vmem, vmem, vmem),
        scratch_shapes=[
            pltpu.VMEM((n, 2, slot, cols), BF16),
            pltpu.VMEM((2, n, slot, width), BF16),
            pltpu.VMEM((hid, width), BF16),
            pltpu.VMEM((hid, width), BF16),
            pltpu.VMEM((hid, width), BF16),
            pltpu.VMEM((total, toks), BF16),
            pltpu.VMEM((2, total, hid), BF16),
            pltpu.VMEM((3, hid, total), BF16),
            pltpu.VMEM((3, hid, width), BF16),
            pltpu.VMEM((hid, 128), F32),
            pltpu.VMEM((2, total, cols), BF16),
            pltpu.VMEM((2, total, cols), BF16),
            pltpu.VMEM((total, cols), F32),
            pltpu.VMEM((n, slot, cols), F32),
            pltpu.VMEM((n, slot, cols), BF16),
            pltpu.VMEM((n, slot, cols), BF16),
            pltpu.VMEM((n, slot, cols), BF16),
            pltpu.VMEM((n, slot, cols), BF16),
            pltpu.VMEM((t, 1, total), F32),
            pltpu.VMEM((1, total), F32),
            pltpu.VMEM((n, 1, total), F32),
            pltpu.VMEM((t, part, sh), BF16),
            pltpu.VMEM((t, n, part, sh), BF16),
            pltpu.VMEM((n, part, cut), BF16),
            pltpu.VMEM((t, n, part, cut), BF16),
            pltpu.VMEM((n, 1, sh), F32),
            pltpu.VMEM((toks, cols), BF16),
            pltpu.VMEM((toks, cols), BF16),
            pltpu.VMEM((part, width), BF16),
            pltpu.VMEM((toks, sh), BF16),
            dma((4,)),
            dma((3,)), dma((3,)),
            dma((n,)), dma((n,)), dma((n,)), dma((n,)), dma((2, n)), dma((2, n)),
            dma((n,)), dma((n,)), dma((n,)), dma((n,)), dma((t,)), dma((t,)),
            dma((2,)), dma((2,)), dma((n,)), dma((n,)), dma((n,)), dma((n,)),
            dma((t,)), dma((t,)), dma((n,)), dma((n,)), dma((n,)), dma((n,)),
        ],
        compiler_params=pltpu.CompilerParams(
            collective_id=0, has_side_effects=True, vmem_limit_bytes=60 * 1024 * 1024
        ),
    )(
        expert_ids.T, route_weights.T, tokens, out_grad, shared_act, gate_proj, up_proj, down_proj
    )
    count = len(results)
    token_grad, route, gate, up, down, norms, shared, snorm = pl.pallas_call(
        hand_over,
        out_shape=[jax.ShapeDtypeStruct(r.shape, r.dtype) for r in results],
        in_specs=[hbm] * count,
        out_specs=[hbm] * count,
        scratch_shapes=[pltpu.VMEM(r.shape, r.dtype) for r in results]
        + [dma((2 * count,)), dma((2 * count,))],
    )(*results)
    return (
        token_grad, route.T, gate[None], up[None], down[None], norms.transpose(1, 0, 2), shared,
        snorm[0],
    )


def local(tokens, out_grad, expert_ids, route_weights, gate_proj, up_proj, down_proj, shared_act):
    n = lax.axis_size("ep")
    t = lax.axis_size("tp")
    toks, width = tokens.shape
    hid = gate_proj.shape[1]
    slot = -(-(5 * toks * expert_ids.shape[1] // (4 * n)) // 16) * 16
    fits = (
        gate_proj.shape[0] == 1 and expert_ids.shape[1] == 2 and t == 4 and n in (2, 4, 8, 16, 32, 64, 128)
        and toks % 128 == 0 and toks // t % 16 == 0 and width // t % 128 == 0
        and hid % 256 == 0 and n * slot % 128 == 0 and width // n % 128 == 0
        and shared_act.shape[1] // t % 128 == 0
    )
    body = fused if fits else plain
    return body(
        tokens, out_grad, expert_ids, route_weights, gate_proj, up_proj, down_proj, shared_act
    )


def solution(mesh):
    placed = (
        P("ep", None),
        P("ep", None),
        P("ep", None),
        P("ep", None),
        P("ep", "tp", None),
        P("ep", "tp", None),
        P("ep", "tp", None),
        P("ep", None),
    )
    return jax.shard_map(
        local,
        mesh=mesh,
        in_specs=placed,
        out_specs=(
            P("ep", "tp"),
            P("ep", None),
            P("ep", "tp", None),
            P("ep", "tp", None),
            P("ep", "tp", None),
            P("ep", None, "tp"),
            P("tp", "ep"),
            P("tp"),
        ),
        check_vma=False,
    )
```

profile of v0, /device:TPU:0, one launch (start us, length us, event | category | flops | bytes accessed | tf_op | source)
XLA Modules:
  0.0 65.2 jit_solution(6103996950844669439)
XLA Ops:
  0.6 58.6 %shard_map.143 = (bf16[128,512]{1,0:T(8,128)(2,1)}, f32[2,128]{1,0:T(2,128)}, bf16[512,2048]{1,0:T(8,128)(2,1)}, bf16[512,2048]{1,0:T(8,128)(2,1)}, bf16[512,204...) custom-call(s32[2,128]{1,0:T(2,128)} %bitcast.8, f32[2,128]{1,0:T(2,128)} %bitcast.9, ...), custom_call_target="tpu_custom_call" | custom-call | tf_op jit(solution)/shard_map/pallas_call | solution.py:551
  59.3 5.9 %shard_map.144 = (bf16[128,512]{1,0:T(8,128)(2,1)}, f32[2,128]{1,0:T(2,128)}, bf16[512,2048]{1,0:T(8,128)(2,1)}, bf16[512,2048]{1,0:T(8,128)(2,1)}, bf16[512,204...) custom-call(bf16[128,512]{1,0:T(8,128)(2,1)} %get-tuple-element.24.refs_0_, ...), custom_call_target="tpu_custom_call" | custom-call | tf_op jit(solution)/shard_map/pallas_call | solution.py:610
where the time goes:
time: 66.2 us; the launch traced here: 65.2 us
  Pallas kernels  64.6 us (98%)
    pallas_call x1, Pallas kernels, fused(): pl.pallas_call(functools.partial(kernel, n, t, cap, slot), out_shape=(jax...  58.6 us
    pallas_call x1, Pallas kernels, fused(): pl.pallas_call(hand_over, out_shape=[jax.ShapeDtypeStruct(r.shape, r.dtyp...  5.94 us

commit v1 on v0

--- a/solution.py
+++ b/solution.py
@@ -155,11 +155,11 @@
     n, t, cap, slot,
     ids_ref, rw_ref, tok_hbm, og_hbm, act_hbm, wg_hbm, wu_hbm, wd_hbm,
     token_out, route_out, gate_out, up_out, down_out, norms_out, shared_out, snorm_out,
-    send, rows, wg, wu, wd, picks, delta, turned, grads, squares,
+    send, rows, wg, wu, wd, picks, delta, turned, squares,
     pair_send, pair_recv, acc_far, acc_own, far_send, far_recv, back_send, back_recv,
     inner_tp, inner_tot, inner_ep, act_send, act_all, og_send, og_all, snorm_all,
     tok_part, og_part, og_mine, act_part, l_sem,
-    w_sem, g_sem, d_s, d_r, m_s, m_r, c_s, c_r, a_s, a_r, o_s, o_r, q_s, q_r,
+    w_sem, d_s, d_r, m_s, m_r, c_s, c_r, a_s, a_r, o_s, o_r, q_s, q_r,
     p_s, p_r, f_s, f_r, b_s, b_r, i_s, i_r, j_s, j_r, n_s, n_r,
 ):
     me = lax.axis_index("ep")
@@ -421,7 +421,7 @@
                 turned[j], rows[source, :, :, at].reshape(total, block),
                 preferred_element_type=F32,
             )
-            grads[j, :, at] = value.astype(BF16)
+            (gate_out, up_out, down_out)[j][:, at] = value.astype(BF16)
             sq = value * value
             here = squares[...]
             for k in range(block // 128):
@@ -432,12 +432,7 @@
         lax.fori_loop(0, width // block, step, 0)
         norms_out[j] = column_to_row(jnp.sum(squares[...], 1, keepdims=True))
 
-    outs = [
-        pltpu.make_async_copy(grads.at[j], out, g_sem.at[j])
-        for j, out in enumerate((gate_out, up_out, down_out))
-    ]
     grad_of(0, 0)
-    outs[0].start()
     for i in range(1, t):
         og_spread(i).wait_recv()
     shared = lax.dot_general(
@@ -455,9 +450,7 @@
     for i in range(1, n):
         snorm_copy(i).start()
     grad_of(1, 0)
-    outs[1].start()
     grad_of(2, 1)
-    outs[2].start()
 
     for i in range(1, n):
         inner_back(i).wait_recv()
@@ -501,35 +494,17 @@
         inner_copy(i).wait_send()
     pair_copy(0).wait_send()
     pair_copy(1).wait_send()
-    for out in outs:
-        out.wait()
 
 
 def hand_over(*refs):
-    count = (len(refs) - 2) // 3
-    sources, targets, held = refs[:count], refs[count : 2 * count], refs[2 * count : 3 * count]
-    in_sem, out_sem = refs[-2:]
-    order = sorted(range(count), key=lambda j: sources[j].size)
-    taken, given = [], []
-    for j in order:
-        top = sources[j].shape[0]
-        pieces = 2 if top % 256 == 0 else 1
-        for k in range(pieces):
-            at = pl.ds(k * (top // pieces), top // pieces)
-            sem = 2 * j + k
-            taken.append(
-                pltpu.make_async_copy(sources[j].at[at], held[j].at[at], in_sem.at[sem])
-            )
-            given.append(
-                pltpu.make_async_copy(held[j].at[at], targets[j].at[at], out_sem.at[sem])
-            )
-    for move in taken:
-        move.start()
-    for move, after in zip(taken, given):
+    count = (len(refs) - 1) // 2
+    sources, targets, sem = refs[:count], refs[count : 2 * count], refs[-1]
+    moves = []
+    for j in sorted(range(count), key=lambda j: sources[j].size):
+        moves.append(pltpu.make_async_copy(sources[j], targets[j], sem.at[j]))
+        moves[-1].start()
+    for move in moves:
         move.wait()
-        after.start()
-    for after in given:
-        after.wait()
 
 
 def fused(tokens, out_grad, expert_ids, route_weights, gate_proj, up_proj, down_proj, shared_act):
@@ -551,17 +526,17 @@
     results = pl.pallas_call(
         functools.partial(kernel, n, t, cap, slot),
         out_shape=(
-            jax.ShapeDtypeStruct((toks, cols), BF16),
-            jax.ShapeDtypeStruct((2, toks), F32),
-            jax.ShapeDtypeStruct((hid, width), BF16),
-            jax.ShapeDtypeStruct((hid, width), BF16),
-            jax.ShapeDtypeStruct((hid, width), BF16),
-            jax.ShapeDtypeStruct((3, 1, hid), F32),
-            jax.ShapeDtypeStruct((sh, cut), F32),
-            jax.ShapeDtypeStruct((1, sh), F32),
+            pltpu.VMEM((toks, cols), BF16),
+            pltpu.VMEM((2, toks), F32),
+            pltpu.VMEM((hid, width), BF16),
+            pltpu.VMEM((hid, width), BF16),
+            pltpu.VMEM((hid, width), BF16),
+            pltpu.VMEM((3, 1, hid), F32),
+            pltpu.VMEM((sh, cut), F32),
+            pltpu.VMEM((1, sh), F32),
         ),
         in_specs=[vmem] * 2 + [hbm] * 6,
-        out_specs=(vmem, vmem, hbm, hbm, hbm, vmem, vmem, vmem),
+        out_specs=(vmem,) * 8,
         scratch_shapes=[
             pltpu.VMEM((n, 2, slot, cols), BF16),
             pltpu.VMEM((2, n, slot, width), BF16),
@@ -571,7 +546,6 @@
             pltpu.VMEM((total, toks), BF16),
             pltpu.VMEM((2, total, hid), BF16),
             pltpu.VMEM((3, hid, total), BF16),
-            pltpu.VMEM((3, hid, width), BF16),
             pltpu.VMEM((hid, 128), F32),
             pltpu.VMEM((2, total, cols), BF16),
             pltpu.VMEM((2, total, cols), BF16),
@@ -594,27 +568,33 @@
             pltpu.VMEM((part, width), BF16),
             pltpu.VMEM((toks, sh), BF16),
             dma((4,)),
-            dma((3,)), dma((3,)),
+            dma((3,)),
             dma((n,)), dma((n,)), dma((n,)), dma((n,)), dma((2, n)), dma((2, n)),
             dma((n,)), dma((n,)), dma((n,)), dma((n,)), dma((t,)), dma((t,)),
             dma((2,)), dma((2,)), dma((n,)), dma((n,)), dma((n,)), dma((n,)),
             dma((t,)), dma((t,)), dma((n,)), dma((n,)), dma((n,)), dma((n,)),
         ],
         compiler_params=pltpu.CompilerParams(
-            collective_id=0, has_side_effects=True, vmem_limit_bytes=60 * 1024 * 1024
+            collective_id=0, has_side_effects=True, vmem_limit_bytes=36 * 1024 * 1024
         ),
     )(
-        expert_ids.T, route_weights.T, tokens, out_grad, shared_act, gate_proj, up_proj, down_proj
+        *[
+            pltpu.with_memory_space_constraint(r, pltpu.HBM)
+            for r in (
+                expert_ids.T, route_weights.T, tokens, out_grad, shared_act, gate_proj, up_proj,
+                down_proj,
+            )
+        ]
     )
     count = len(results)
     token_grad, route, gate, up, down, norms, shared, snorm = pl.pallas_call(
         hand_over,
         out_shape=[jax.ShapeDtypeStruct(r.shape, r.dtype) for r in results],
-        in_specs=[hbm] * count,
+        in_specs=[vmem] * count,
         out_specs=[hbm] * count,
-        scratch_shapes=[pltpu.VMEM(r.shape, r.dtype) for r in results]
-        + [dma((2 * count,)), dma((2 * count,))],
-    )(*results)
+        scratch_shapes=[dma((count,))],
+        compiler_params=pltpu.CompilerParams(vmem_limit_bytes=4 * 1024 * 1024),
+    )(*[pltpu.with_memory_space_constraint(r, pltpu.VMEM) for r in results])
     return (
         token_grad, route.T, gate[None], up[None], down[None], norms.transpose(1, 0, 2), shared,
         snorm[0],

time: 66.2 us -> 62.3 us (0.941)
  Pallas kernels: 64.6 us -> 60.7 us
    pallas_call x1, Pallas kernels: 5.94 us -> 2.91 us  [fused(): pl.pallas_call(hand_over, out_shape=[jax.ShapeDtypeStruct(r.shape, r.dtyp...]
    pallas_call x1, Pallas kernels: 58.6 us -> 57.8 us  [fused(): pl.pallas_call(functools.partial(kernel, n, t, cap, slot), out_shape=(plt...]
where the time goes in v1:
time: 62.3 us; the launch traced here: 61.4 us
  Pallas kernels  60.7 us (97%)
  between operations  0.64 us (1%)
    pallas_call x1, Pallas kernels, fused(): pl.pallas_call(functools.partial(kernel, n, t, cap, slot), out_shape=(plt...  57.8 us
    pallas_call x1, Pallas kernels, fused(): pl.pallas_call(hand_over, out_shape=[jax.ShapeDtypeStruct(r.shape, r.dtyp...  2.91 us

profile of v1, /device:TPU:0, one launch (start us, length us, event | category | flops | bytes accessed | tf_op | source)
XLA Modules:
  0.0 61.4 jit_solution(435033447339692075)
XLA Ops:
  0.6 57.8 %shard_map.143 = (bf16[128,512]{1,0:T(8,128)(2,1)S(1)}, f32[2,128]{1,0:T(2,128)S(1)}, bf16[512,2048]{1,0:T(8,128)(2,1)S(1)}, bf16[512,2048]{1,0:T(8,128)(2,1)S(1...) custom-call(s32[2,128]{1,0:T(2,128)} %bitcast.8, ...), custom_call_target="tpu_custom_call" | custom-call | tf_op jit(solution)/shard_map/pallas_call | solution.py:526
  58.5 2.9 %shard_map.144 = (bf16[128,512]{1,0:T(8,128)(2,1)}, f32[2,128]{1,0:T(2,128)}, bf16[512,2048]{1,0:T(8,128)(2,1)}, bf16[512,2048]{1,0:T(8,128)(2,1)}, bf16[512,204...) custom-call(bf16[128,512]{1,0:T(8,128)(2,1)S(1)} %get-tuple-element.24.refs_0_, ...), custom_call_target="tpu_custom_call" | custom-call | tf_op jit(solution)/shard_map/pallas_call | solution.py:590

commit v2 on v1

v2 whole, which is shorter than its diff:
```python
import functools

import jax
import jax.numpy as jnp
from jax import lax
from jax.experimental import pallas as pl
from jax.experimental.pallas import tpu as pltpu
from jax.sharding import PartitionSpec as P


def plain(tokens, out_grad, expert_ids, route_weights, gate_proj, up_proj, down_proj, shared_act):
    ep_count = lax.axis_size("ep")
    tp_count = lax.axis_size("tp")
    tok_count, model_width = tokens.shape
    top_count = expert_ids.shape[1]
    exp_local = gate_proj.shape[0]
    experts = exp_local * ep_count
    capacity = 5 * tok_count * top_count // (4 * experts)
    slot_count = experts * capacity
    assign = tok_count * top_count
    columns = model_width // tp_count
    offset = lax.axis_index("tp") * columns
    flat_expert = expert_ids.reshape(assign)
    onehot = (flat_expert[:, None] == jnp.arange(experts, dtype=jnp.int32)[None, :]).astype(
        jnp.float32
    )
    earlier = (jnp.arange(assign)[:, None] > jnp.arange(assign)[None, :]).astype(jnp.float32)
    counted = jnp.dot(earlier, onehot, precision=lax.Precision.HIGHEST)
    rank_in = jnp.sum(counted * onehot, 1).astype(jnp.int32)
    slot_id = flat_expert * capacity + rank_in
    picked = (jnp.arange(slot_count, dtype=jnp.int32)[:, None] == slot_id[None, :]).astype(
        jnp.float32
    )
    source_id = jnp.dot(
        picked, jnp.arange(assign, dtype=jnp.float32), precision=lax.Precision.HIGHEST
    ).astype(jnp.int32)
    filled = jnp.sum(picked, 1) > 0.5
    scaled = (
        (route_weights[:, :, None] * out_grad[:, None, :])
        .astype(jnp.bfloat16)
        .reshape(assign, model_width)
    )

    def slot_rows(source_rows, row_index):
        taken = jnp.take(source_rows, row_index, axis=0)
        return jnp.where(filled[:, None], taken, jnp.zeros((), source_rows.dtype))

    token_part = lax.dynamic_slice_in_dim(tokens, offset, columns, 1)
    scaled_part = lax.dynamic_slice_in_dim(scaled, offset, columns, 1)
    send_in = slot_rows(token_part, source_id // top_count).reshape(
        ep_count, exp_local, capacity, columns
    )
    send_cot = slot_rows(scaled_part, source_id).reshape(ep_count, exp_local, capacity, columns)
    part_in, part_cot = (
        lax.all_to_all(send_in, "ep", split_axis=0, concat_axis=2, tiled=True),
        lax.all_to_all(send_cot, "ep", split_axis=0, concat_axis=2, tiled=True),
    )
    joined_in, joined_cot = (
        lax.all_gather(part_in, "tp", axis=3, tiled=True),
        lax.all_gather(part_cot, "tp", axis=3, tiled=True),
    )
    rows_in = joined_in[0]
    rows_cot = joined_cot[0]
    gate_pre = jnp.einsum("erd,efd->erf", rows_in, gate_proj, preferred_element_type=jnp.float32)
    up_pre = jnp.einsum("erd,efd->erf", rows_in, up_proj, preferred_element_type=jnp.float32)
    sigmoid_a = jax.nn.sigmoid(gate_pre)
    silu_a = gate_pre * sigmoid_a
    hidden = (silu_a * up_pre).astype(jnp.bfloat16)
    hidden_grad = jnp.einsum(
        "erd,efd->erf", rows_cot, down_proj, preferred_element_type=jnp.float32
    )
    up_delta = (hidden_grad * silu_a).astype(jnp.bfloat16)
    gate_delta = (hidden_grad * up_pre * sigmoid_a * (1.0 + gate_pre * (1.0 - sigmoid_a))).astype(
        jnp.bfloat16
    )
    gate_full = jnp.einsum("erf,erd->efd", gate_delta, rows_in, preferred_element_type=jnp.float32)
    up_full = jnp.einsum("erf,erd->efd", up_delta, rows_in, preferred_element_type=jnp.float32)
    down_full = jnp.einsum("erf,erd->efd", hidden, rows_cot, preferred_element_type=jnp.float32)
    row_norms = jnp.stack(
        [
            jnp.sum(gate_full * gate_full, 2),
            jnp.sum(up_full * up_full, 2),
            jnp.sum(down_full * down_full, 2),
        ],
        axis=1,
    )
    row_total = rows_in.shape[1]
    partial_value = jnp.einsum(
        "erf,efd->erd", gate_delta, gate_proj, preferred_element_type=jnp.float32
    )
    partial_value = partial_value + jnp.einsum(
        "erf,efd->erd", up_delta, up_proj, preferred_element_type=jnp.float32
    )
    partials = partial_value.astype(jnp.bfloat16).reshape(exp_local, row_total, tp_count, columns)
    inner_part = jnp.sum(hidden.astype(jnp.float32) * hidden_grad, 2).astype(jnp.bfloat16)
    inner_parts = jnp.broadcast_to(inner_part[:, :, None], (exp_local, row_total, tp_count))
    received, received_inner = (
        lax.all_to_all(partials, "tp", split_axis=2, concat_axis=2, tiled=True),
        lax.all_to_all(inner_parts, "tp", split_axis=2, concat_axis=2, tiled=True),
    )
    slot_grad = jnp.sum(received.astype(jnp.float32), 2)
    inner = jnp.sum(received_inner.astype(jnp.float32), 2)
    returned, returned_inner = (
        lax.all_to_all(
            slot_grad.reshape(exp_local, ep_count, capacity, columns),
            "ep",
            split_axis=1,
            concat_axis=0,
            tiled=True,
        ),
        lax.all_to_all(
            inner.reshape(exp_local, ep_count, capacity),
            "ep",
            split_axis=1,
            concat_axis=0,
            tiled=True,
        ),
    )
    slot_back = returned.reshape(slot_count, columns)
    inner_back = returned_inner.reshape(slot_count)
    token_grad = jnp.take(slot_back, slot_id, axis=0).reshape(tok_count, top_count, columns).sum(1)
    route_grad = jnp.take(inner_back, slot_id).reshape(tok_count, top_count) / route_weights
    shared_rows = shared_act.shape[1] // tp_count
    shared_part = lax.dynamic_slice_in_dim(
        shared_act, lax.axis_index("tp") * shared_rows, shared_rows, 1
    )
    shared_term = lax.dot_general(
        shared_part, out_grad, (((0,), (0,)), ((), ())), preferred_element_type=jnp.float32
    )
    shared_grad = lax.psum_scatter(shared_term, "ep", scatter_dimension=1, tiled=True)
    shared_norms = lax.psum(jnp.sum(shared_grad * shared_grad, 1), "ep")
    return (
        token_grad.astype(jnp.bfloat16),
        route_grad,
        gate_full.astype(jnp.bfloat16),
        up_full.astype(jnp.bfloat16),
        down_full.astype(jnp.bfloat16),
        row_norms,
        shared_grad,
        shared_norms,
    )


MESH = pl.DeviceIdType.MESH
F32 = jnp.float32
BF16 = jnp.bfloat16
NT = (((1,), (1,)), ((), ()))


def column_to_row(col, width=128):
    return jnp.broadcast_to(col, (col.shape[0], width)).T[0:1]


def kernel(
    n, t, cap, slot,
    ids_hbm, rw_hbm, tok_hbm, og_hbm, act_hbm, wg_hbm, wu_hbm, wd_hbm,
    token_out, route_out, gate_out, up_out, down_out, norms_out, shared_out, snorm_out,
    send, rows, wg, wu, wd, picks, place, weight_of, delta, turned, squares,
    pair_send, pair_recv, acc_far, acc_own, far_send, far_recv, back_send, back_recv,
    inner_tp, inner_tot, inner_ep, act_all, og_send, og_all, snorm_all,
    ids_ref, rw_ref, tok_part, og_part, tok_full, og_full, l_sem,
    w_sem, d_s, d_r, m_s, m_r, c_s, c_r, a_s, a_r, o_s, o_r, q_s, q_r,
    p_s, p_r, f_s, f_r, b_s, b_r, i_s, i_r, j_s, j_r, n_s, n_r,
):
    me = lax.axis_index("ep")
    p = lax.axis_index("tp")
    half = t // 2
    buddy = p + 1 - 2 * lax.rem(p, 2)
    mirror = lax.rem(p + half, t)
    mirror_buddy = lax.rem(buddy + half, t)
    toks, width = tok_hbm.shape
    cols = width // t
    hid = wg.shape[0]
    total = n * slot
    part = toks // 2
    core = lax.rem(p, 2)
    sh = act_hbm.shape[1] // t
    cut = width // n

    def span(q, size):
        return pl.ds(pl.multiple_of(q * size, 128), size)

    def peer(i):
        out, bit = 0, 1
        while bit < n:
            digit, flip = lax.rem(me // bit, 2), lax.rem(i // bit, 2)
            out = out + bit * (digit + flip - 2 * digit * flip)
            bit *= 2
        return out

    def tp_ahead(i):
        return lax.rem(p + i, t)

    def copy(src, dst, s_sem, r_sem, where):
        return pltpu.make_async_remote_copy(
            src_ref=src, dst_ref=dst, send_sem=s_sem, recv_sem=r_sem,
            device_id=where, device_id_type=MESH,
        )

    local = pltpu.make_async_copy
    loads = [
        local(tok_hbm.at[:, span(p, cols)], tok_part, l_sem.at[0]),
        local(og_hbm.at[:, span(p, cols)], og_part, l_sem.at[1]),
    ]
    own_loads = [
        local(tok_hbm, tok_full, l_sem.at[4]),
        local(og_hbm, og_full, l_sem.at[5]),
    ]
    late_loads = [
        local(
            act_hbm.at[q * part : (q + 1) * part, span(p, sh)], act_all.at[q, 0], l_sem.at[6 + q]
        )
        for q in range(2)
    ]
    for i in range(n):
        target = og_send.at[i] if i else og_all.at[core, 0]
        late_loads.append(
            local(
                og_hbm.at[pl.ds(pl.multiple_of(core * part, 16), part), span(peer(i), cut)],
                target, l_sem.at[8 + i],
            )
        )
    weights = [
        local(wg_hbm.at[0], wg, w_sem.at[0]),
        local(wu_hbm.at[0], wu, w_sem.at[1]),
        local(wd_hbm.at[0], wd, w_sem.at[2]),
    ]
    small_loads = [
        local(ids_hbm, ids_ref, l_sem.at[2]),
        local(rw_hbm, rw_ref, l_sem.at[3]),
    ]
    for load in small_loads + loads:
        load.start()
    barrier = pltpu.get_barrier_semaphore()
    for i in range(1, n):
        pl.semaphore_signal(barrier, inc=1, device_id={"ep": peer(i)}, device_id_type=MESH)
    for i in range(1, t):
        pl.semaphore_signal(barrier, inc=1, device_id={"tp": tp_ahead(i)}, device_id_type=MESH)
    for load in own_loads + weights + late_loads:
        load.start()

    for load in small_loads:
        load.wait()
    expert = lax.broadcasted_iota(jnp.int32, (128, toks), 0)
    first = ids_ref[0:1, :] == expert
    second = ids_ref[1:2, :] == expert
    member = jnp.where(first | second, 1.0, 0.0).astype(F32)
    weight_t = jnp.where(first, rw_ref[0:1, :], jnp.where(second, rw_ref[1:2, :], 0.0))
    upper = lax.broadcasted_iota(jnp.int32, (toks, toks), 0) < lax.broadcasted_iota(
        jnp.int32, (toks, toks), 1
    )
    upper = jnp.where(upper, 1.0, 0.0).astype(BF16)
    rank_t = jnp.dot(member.astype(BF16), upper, preferred_element_type=F32)
    place_t = jnp.where(member > 0.5, rank_t, -1.0)
    place[...] = place_t
    weight_of[...] = weight_t
    row_in = lax.broadcasted_iota(jnp.int32, (slot, toks), 0).astype(F32)
    slot_weight = []
    for i in range(n):
        at = pl.ds(peer(i), 1)
        hit = jnp.where(place[at, :] == row_in, 1.0, 0.0).astype(F32)
        picks[i * slot : (i + 1) * slot, :] = hit.astype(BF16)
        slot_weight.append(jnp.sum(hit * weight_of[at, :], 1, keepdims=True))
    for load in loads:
        load.wait()
    away = pl.ds(slot, total - slot)
    got = jnp.dot(picks[away, :], tok_part[...], preferred_element_type=F32).astype(BF16)
    send[1:, 0] = got.reshape(n - 1, slot, cols)
    got = jnp.dot(picks[away, :], og_part[...], preferred_element_type=F32)
    got = got * jnp.concatenate(slot_weight[1:], 0)
    send[1:, 1] = got.astype(BF16).reshape(n - 1, slot, cols)
    pl.semaphore_wait(barrier, n + t - 2)

    def chunk(i, q):
        return rows.at[:, i, pl.ds(0, cap), span(q, cols)]

    def dispatch(i):
        return copy(
            send.at[i, :, pl.ds(0, cap), :], chunk(i, p), d_s.at[i], d_r.at[i], {"ep": peer(i)}
        )

    def to_mirror(i):
        return copy(chunk(i, p), chunk(i, p), m_s.at[i], m_r.at[i], {"tp": mirror})

    def to_buddy(i):
        return copy(chunk(i, p), chunk(i, p), c_s.at[0, i], c_r.at[0, i], {"tp": buddy})

    def on_buddy(i):
        return copy(
            chunk(i, mirror), chunk(i, mirror), c_s.at[1, i], c_r.at[1, i], {"tp": buddy}
        )

    def act_copy(j):
        low = j & -j
        return copy(
            act_all.at[:, j - low], act_all.at[:, j], a_s.at[j], a_r.at[j], {"ep": peer(low)}
        )

    def act_from(j):
        bit = 1
        while bit < n and (j == 0 or bit < (j & -j)):
            act_copy(j + bit).start()
            bit *= 2

    def og_copy(i):
        return copy(og_send.at[i], og_all.at[core, i], o_s.at[i], o_r.at[i], {"ep": peer(i)})

    def og_buddy():
        return copy(og_all.at[core], og_all.at[core], q_s, q_r, {"tp": buddy})

    def inner_copy(i):
        return copy(inner_tp.at[p], inner_tp.at[p], i_s.at[i], i_r.at[i], {"tp": tp_ahead(i)})

    def inner_back(i):
        return copy(inner_tot, inner_ep.at[i], j_s.at[i], j_r.at[i], {"ep": peer(i)})

    def pair_copy(g, k):
        return copy(
            pair_send.at[g, k], pair_recv.at[g, k], p_s.at[g, k], p_r.at[g, k], {"tp": buddy}
        )

    def far_copy(i):
        at = pl.ds(0, cap)
        return copy(
            far_send.at[i, at, :], far_recv.at[i, at, :], f_s.at[i], f_r.at[i], {"tp": mirror}
        )

    def back_copy(i):
        at = pl.ds(0, cap)
        return copy(
            back_send.at[i, at, :], back_recv.at[i, at, :], b_s.at[i], b_r.at[i], {"ep": peer(i)}
        )

    def snorm_copy(i):
        return copy(snorm_all.at[0], snorm_all.at[i], n_s.at[i], n_r.at[i], {"ep": peer(i)})

    near = list(range(n // 2))
    distant = list(range(n // 2, n))
    groups = (near, distant)
    height = n // 2 * slot
    tile = min(hid, 256)

    for i in range(1, n):
        dispatch(i).start()
    for load in own_loads:
        load.wait()
    if slot != cap:
        rows[:, 1:, cap:, :] = jnp.zeros((2, n - 1, slot - cap, width), BF16)
        back_recv[:, cap:, :] = jnp.zeros((n, slot - cap, cols), BF16)
    rows[0, 0] = jnp.dot(picks[0:slot, :], tok_full[...], preferred_element_type=F32).astype(BF16)
    got = jnp.dot(picks[0:slot, :], og_full[...], preferred_element_type=F32)
    rows[1, 0] = (got * slot_weight[0]).astype(BF16)

    def pass_on(i):
        dispatch(i).wait_recv()
        to_mirror(i).start()
        to_buddy(i).start()

    def from_mirror(i):
        to_mirror(i).wait_recv()
        on_buddy(i).start()

    def settle(i):
        to_buddy(i).wait_recv()
        on_buddy(i).wait_recv()

    def forward(g, f):
        sources = slice(groups[g][0], groups[g][-1] + 1)
        at = slice(f * tile, (f + 1) * tile)
        x_in = rows[0, sources].reshape(height, width)
        x_cot = rows[1, sources].reshape(height, width)
        gate_pre = lax.dot_general(wg[at, :], x_in, NT, preferred_element_type=F32)
        up_pre = lax.dot_general(wu[at, :], x_in, NT, preferred_element_type=F32)
        hidden_grad = lax.dot_general(wd[at, :], x_cot, NT, preferred_element_type=F32)
        sig = jax.nn.sigmoid(gate_pre)
        silu = gate_pre * sig
        hidden = (silu * up_pre).astype(BF16)
        up_d = (hidden_grad * silu).astype(BF16)
        gate_d = (hidden_grad * up_pre * sig * (1.0 + gate_pre * (1.0 - sig))).astype(BF16)
        turned[g, 0, at, :] = gate_d
        turned[g, 1, at, :] = up_d
        turned[g, 2, at, :] = hidden
        delta[g, 0, :, at] = gate_d.T
        delta[g, 1, :, at] = up_d.T
        part_inner = jnp.sum(hidden.astype(F32) * hidden_grad, 0, keepdims=True)
        inner_tp[p, g] = part_inner if f == 0 else inner_tp[p, g] + part_inner

    def share(g, q):
        at = span(q, cols)
        value = jnp.dot(delta[g, 0], wg[:, at], preferred_element_type=F32)
        return value + jnp.dot(delta[g, 1], wu[:, at], preferred_element_type=F32)

    def shares_far(g):
        pair_send[g, 0] = share(g, mirror_buddy).astype(BF16)
        pair_copy(g, 0).start()
        acc_far[...] = share(g, mirror)
        pair_send[g, 1] = share(g, buddy).astype(BF16)
        pair_copy(g, 1).start()
        pair_copy(g, 0).wait_recv()
        far = (acc_far[...] + pair_recv[g, 0].astype(F32)).astype(BF16)
        far_send[groups[g][0] : groups[g][-1] + 1] = far.reshape(n // 2, slot, cols)

    def far_start(g):
        for i in order[g]:
            far_copy(i).start()

    def shares_own(g):
        value = share(g, p)
        pair_copy(g, 1).wait_recv()
        value = value + pair_recv[g, 1].astype(F32)
        acc_own[groups[g][0] : groups[g][-1] + 1] = value.reshape(n // 2, slot, cols)

    def give_back(i):
        far_copy(i).wait_recv()
        value = (acc_own[i, 0:cap] + far_recv[i, 0:cap].astype(F32)).astype(BF16)
        if isinstance(i, int) and i == 0:
            back_recv[0, 0:cap] = value
        else:
            back_send[i, 0:cap] = value
            back_copy(i).start()

    order = (near[1:] + near[:1], distant)
    steps = hid // tile

    ahead = near[1:] + distant[:1]
    for i in ahead:
        pass_on(i)
    for i in near[1:]:
        from_mirror(i)
    for w in weights:
        w.wait()
    for i in near[1:]:
        settle(i)
    rest = distant[1:]
    tiles = [f for f in range(steps)]
    for k, i in enumerate(rest):
        pass_on(i)
        if k == len(rest) - 1:
            count = len(tiles)
        else:
            count = max(1, steps // (len(rest) - 1))
        for f in tiles[:count]:
            forward(0, f)
        del tiles[:count]
        from_mirror(distant[k])
    for load in late_loads:
        load.wait()
    act_from(0)
    for j in distant + near[1:]:
        og_copy(j).start()
    shares_far(0)
    from_mirror(distant[-1])
    far_start(0)
    shares_own(0)
    for i in distant:
        settle(i)

    for f in range(steps):
        forward(1, f)
    for i in range(1, t):
        inner_copy(i).start()
    shares_far(1)
    far_start(1)
    levels = [1 << k for k in reversed(range(n.bit_length() - 1))]

    def act_level(low):
        for j in range(low, n, 2 * low):
            act_copy(j).wait_recv()
            act_from(j)

    act_level(levels[0])
    middle = [j for low in levels[1:-1] for j in range(low, n, 2 * low)]

    def act_next(count):
        for j in middle[:count]:
            act_copy(j).wait_recv()
            act_from(j)
        del middle[:count]

    act_next(1)
    for i in order[0]:
        give_back(i)
    shares_own(1)

    block = min(width, 512)
    chunks = width // block

    def grad_of(j, lo, hi):
        out = (gate_out, up_out, down_out)[j]
        source = j // 2

        def step(c, carry):
            at = pl.ds(pl.multiple_of(c * block, block), block)
            value = jnp.dot(
                turned[0, j], rows[source, 0 : n // 2, :, at].reshape(height, block),
                preferred_element_type=F32,
            )
            value = value + jnp.dot(
                turned[1, j], rows[source, n // 2 :, :, at].reshape(height, block),
                preferred_element_type=F32,
            )
            out[:, at] = value.astype(BF16)
            sq = value * value
            here = squares[j]
            for k in range(block // 128):
                here = here + sq[:, k * 128 : (k + 1) * 128]
            squares[j] = here
            return carry

        lax.fori_loop(lo, hi, step, 0)

    squares[...] = jnp.zeros_like(squares)
    todo = [(j, c) for j in range(3) for c in range(chunks)]

    def spend(count):
        for j, c in todo[:count]:
            grad_of(j, c, c + 1)
        del todo[:count]

    for i in range(1, t):
        inner_copy(i).wait_recv()
    inner_tot[...] = jnp.sum(inner_tp[...], 0)
    inner_ep[0] = inner_tot[...]
    for i in range(1, n):
        inner_back(i).start()
    for k, i in enumerate(order[1]):
        spend(1)
        give_back(i)
        if k:
            act_next(1)
    act_next(len(middle))
    spend(len(todo))
    for j in range(3):
        norms_out[j] = column_to_row(jnp.sum(squares[j], 1, keepdims=True))
    for i in range(1, n):
        og_copy(i).wait_recv()
    og_buddy().start()
    act_level(levels[-1])
    og_buddy().wait_recv()
    shared = lax.dot_general(
        act_all[...].reshape(n * toks, sh), og_all[...].reshape(n * toks, cut),
        (((0,), (0,)), ((), ())), preferred_element_type=F32,
    )
    shared_out[...] = shared
    snorm_all[0] = column_to_row(jnp.sum(shared * shared, 1, keepdims=True))
    for i in range(1, n):
        snorm_copy(i).start()
    for i in range(1, n):
        inner_back(i).wait_recv()
    found = jnp.zeros((n, toks), F32)
    for g in range(2):
        block_of = lax.broadcasted_iota(jnp.int32, (n, height), 1) // slot + g * n // 2
        row_of = lax.broadcasted_iota(jnp.int32, (n, height), 0)
        spread = jnp.zeros((n, height), F32)
        for i in groups[g]:
            spread = jnp.where((block_of == i) & (row_of == i), inner_ep[i, g], spread)
        found = found + jnp.dot(
            spread, picks[g * height : (g + 1) * height, :].astype(F32),
            precision=lax.Precision.HIGHEST, preferred_element_type=F32,
        )
    for k in range(2):
        value = jnp.zeros((1, toks), F32)
        for i in range(n):
            value = value + jnp.where(ids_ref[k : k + 1, :] == peer(i), found[i : i + 1], 0.0)
        route_out[k : k + 1, :] = value / rw_ref[k : k + 1, :]
    for i in range(1, n):
        back_copy(i).wait_recv()
    token_out[...] = lax.dot_general(
        picks[...], back_recv[...].reshape(total, cols), (((0,), (0,)), ((), ())),
        preferred_element_type=F32,
    ).astype(BF16)
    for i in range(1, n):
        snorm_copy(i).wait_recv()
    snorm_out[...] = jnp.sum(snorm_all[...], 0)

    for i in range(1, n):
        dispatch(i).wait_send()
        to_mirror(i).wait_send()
    for i in range(1, n):
        to_buddy(i).wait_send()
        on_buddy(i).wait_send()
        og_copy(i).wait_send()
        act_copy(i).wait_send()
        inner_back(i).wait_send()
        back_copy(i).wait_send()
        snorm_copy(i).wait_send()
    for i in range(n):
        far_copy(i).wait_send()
    for i in range(1, t):
        inner_copy(i).wait_send()
    og_buddy().wait_send()
    for g in range(2):
        for k in range(2):
            pair_copy(g, k).wait_send()


def hand_over(*refs):
    count = (len(refs) - 1) // 2
    sources, targets, sem = refs[:count], refs[count : 2 * count], refs[-1]
    moves = []
    for j in sorted(range(count), key=lambda j: sources[j].size):
        moves.append(pltpu.make_async_copy(sources[j], targets[j], sem.at[j]))
        moves[-1].start()
    for move in moves:
        move.wait()


def fused(tokens, out_grad, expert_ids, route_weights, gate_proj, up_proj, down_proj, shared_act):
    n = lax.axis_size("ep")
    t = lax.axis_size("tp")
    toks, width = tokens.shape
    experts = gate_proj.shape[0] * n
    cap = 5 * toks * expert_ids.shape[1] // (4 * experts)
    slot = -(-cap // 16) * 16
    hid = gate_proj.shape[1]
    cols = width // t
    sh = shared_act.shape[1] // t
    cut = width // n
    part = toks // 2
    total = n * slot
    height = total // 2
    vmem = pl.BlockSpec(memory_space=pltpu.VMEM)
    hbm = pl.BlockSpec(memory_space=pl.ANY)
    dma = pltpu.SemaphoreType.DMA
    results = pl.pallas_call(
        functools.partial(kernel, n, t, cap, slot),
        out_shape=(
            pltpu.VMEM((toks, cols), BF16),
            pltpu.VMEM((2, toks), F32),
            pltpu.VMEM((hid, width), BF16),
            pltpu.VMEM((hid, width), BF16),
            pltpu.VMEM((hid, width), BF16),
            pltpu.VMEM((3, 1, hid), F32),
            pltpu.VMEM((sh, cut), F32),
            pltpu.VMEM((1, sh), F32),
        ),
        in_specs=[hbm] * 8,
        out_specs=(vmem,) * 8,
        scratch_shapes=[
            pltpu.VMEM((n, 2, slot, cols), BF16),
            pltpu.VMEM((2, n, slot, width), BF16),
            pltpu.VMEM((hid, width), BF16),
            pltpu.VMEM((hid, width), BF16),
            pltpu.VMEM((hid, width), BF16),
            pltpu.VMEM((total, toks), BF16),
            pltpu.VMEM((128, toks), F32),
            pltpu.VMEM((128, toks), F32),
            pltpu.VMEM((2, 2, height, hid), BF16),
            pltpu.VMEM((2, 3, hid, height), BF16),
            pltpu.VMEM((3, hid, 128), F32),
            pltpu.VMEM((2, 2, height, cols), BF16),
            pltpu.VMEM((2, 2, height, cols), BF16),
            pltpu.VMEM((height, cols), F32),
            pltpu.VMEM((n, slot, cols), F32),
            pltpu.VMEM((n, slot, cols), BF16),
            pltpu.VMEM((n, slot, cols), BF16),
            pltpu.VMEM((n, slot, cols), BF16),
            pltpu.VMEM((n, slot, cols), BF16),
            pltpu.VMEM((t, 2, 1, height), F32),
            pltpu.VMEM((2, 1, height), F32),
            pltpu.VMEM((n, 2, 1, height), F32),
            pltpu.VMEM((2, n, part, sh), BF16),
            pltpu.VMEM((n, part, cut), BF16),
            pltpu.VMEM((2, n, part, cut), BF16),
            pltpu.VMEM((n, 1, sh), F32),
            pltpu.VMEM((2, toks), jnp.int32),
            pltpu.VMEM((2, toks), F32),
            pltpu.VMEM((toks, cols), BF16),
            pltpu.VMEM((toks, cols), BF16),
            pltpu.VMEM((toks, width), BF16),
            pltpu.VMEM((toks, width), BF16),
            dma((8 + n,)),
            dma((3,)),
            dma((n,)), dma((n,)), dma((n,)), dma((n,)), dma((2, n)), dma((2, n)),
            dma((n,)), dma((n,)), dma((n,)), dma((n,)), dma, dma,
            dma((2, 2)), dma((2, 2)), dma((n,)), dma((n,)), dma((n,)), dma((n,)),
            dma((t,)), dma((t,)), dma((n,)), dma((n,)), dma((n,)), dma((n,)),
        ],
        compiler_params=pltpu.CompilerParams(
            collective_id=0, has_side_effects=True, vmem_limit_bytes=36 * 1024 * 1024
        ),
    )(
        *[
            pltpu.with_memory_space_constraint(r, pltpu.HBM)
            for r in (
                expert_ids.T, route_weights.T, tokens, out_grad, shared_act, gate_proj, up_proj,
                down_proj,
            )
        ]
    )
    count = len(results)
    token_grad, route, gate, up, down, norms, shared, snorm = pl.pallas_call(
        hand_over,
        out_shape=[jax.ShapeDtypeStruct(r.shape, r.dtype) for r in results],
        in_specs=[vmem] * count,
        out_specs=[hbm] * count,
        scratch_shapes=[dma((count,))],
        compiler_params=pltpu.CompilerParams(vmem_limit_bytes=4 * 1024 * 1024),
    )(*[pltpu.with_memory_space_constraint(r, pltpu.VMEM) for r in results])
    return (
        token_grad, route.T, gate[None], up[None], down[None], norms.transpose(1, 0, 2), shared,
        snorm[0],
    )


def local(tokens, out_grad, expert_ids, route_weights, gate_proj, up_proj, down_proj, shared_act):
    n = lax.axis_size("ep")
    t = lax.axis_size("tp")
    toks, width = tokens.shape
    hid = gate_proj.shape[1]
    slot = -(-(5 * toks * expert_ids.shape[1] // (4 * n)) // 16) * 16
    fits = (
        gate_proj.shape[0] == 1 and expert_ids.shape[1] == 2 and t == 4 and n >= 8 and n & (n - 1) == 0 and n <= 128
        and toks % 128 == 0 and toks % 32 == 0 and width // t % 128 == 0
        and hid % 512 == 0 and n * slot % 128 == 0 and width // n % 128 == 0
        and shared_act.shape[1] // t % 128 == 0
    )
    body = fused if fits else plain
    return body(
        tokens, out_grad, expert_ids, route_weights, gate_proj, up_proj, down_proj, shared_act
    )


def solution(mesh):
    placed = (
        P("ep", None),
        P("ep", None),
        P("ep", None),
        P("ep", None),
        P("ep", "tp", None),
        P("ep", "tp", None),
        P("ep", "tp", None),
        P("ep", None),
    )
    return jax.shard_map(
        local,
        mesh=mesh,
        in_specs=placed,
        out_specs=(
            P("ep", "tp"),
            P("ep", None),
            P("ep", "tp", None),
            P("ep", "tp", None),
            P("ep", "tp", None),
            P("ep", None, "tp"),
            P("tp", "ep"),
            P("tp"),
        ),
        check_vma=False,
    )
```

time: 62.3 us -> 51.3 us (0.82); the launches traced: 61.4 us -> 51.1 us
  Pallas kernels: 60.7 us -> 50.5 us
    pallas_call x1, Pallas kernels: 57.8 us -> 47.5 us  [fused(): pl.pallas_call(functools.partial(kernel, n, t, cap, slot), out_shape=(plt...]
where the time goes in v2:
time: 51.3 us; the launch traced here: 51.1 us
  Pallas kernels  50.5 us (98%)
  between operations  0.64 us (1%)
    pallas_call x1, Pallas kernels, fused(): pl.pallas_call(functools.partial(kernel, n, t, cap, slot), out_shape=(plt...  47.5 us
    pallas_call x1, Pallas kernels, fused(): pl.pallas_call(hand_over, out_shape=[jax.ShapeDtypeStruct(r.shape, r.dtyp...  2.91 us

profile of v2, /device:TPU:0, one launch (start us, length us, event | category | flops | bytes accessed | tf_op | source)
XLA Modules:
  0.0 51.1 jit_solution(15322195365572422014)
XLA Ops:
  0.6 47.5 %shard_map.143 = (bf16[128,512]{1,0:T(8,128)(2,1)S(1)}, f32[2,128]{1,0:T(2,128)S(1)}, bf16[512,2048]{1,0:T(8,128)(2,1)S(1)}, bf16[512,2048]{1,0:T(8,128)(2,1)S(1...) custom-call(s32[2,128]{1,0:T(2,128)} %bitcast.8, ...), custom_call_target="tpu_custom_call" | custom-call | tf_op jit(solution)/shard_map/pallas_call | solution.py:625
  48.2 2.9 %shard_map.144 = (bf16[128,512]{1,0:T(8,128)(2,1)}, f32[2,128]{1,0:T(2,128)}, bf16[512,2048]{1,0:T(8,128)(2,1)}, bf16[512,2048]{1,0:T(8,128)(2,1)}, bf16[512,204...) custom-call(bf16[128,512]{1,0:T(8,128)(2,1)S(1)} %get-tuple-element.24.refs_0_, ...), custom_call_target="tpu_custom_call" | custom-call | tf_op jit(solution)/shard_map/pallas_call | solution.py:692

commit v3 on v2

--- a/solution.py
+++ b/solution.py
@@ -155,7 +155,7 @@
     n, t, cap, slot,
     ids_hbm, rw_hbm, tok_hbm, og_hbm, act_hbm, wg_hbm, wu_hbm, wd_hbm,
     token_out, route_out, gate_out, up_out, down_out, norms_out, shared_out, snorm_out,
-    send, rows, wg, wu, wd, picks, place, weight_of, delta, turned, squares,
+    send, rows, wg, wu, wd, picks, place, weight_of, delta_a, delta_b, turned_a, turned_b, squares,
     pair_send, pair_recv, acc_far, acc_own, far_send, far_recv, back_send, back_recv,
     inner_tp, inner_tot, inner_ep, act_all, og_send, og_all, snorm_all,
     ids_ref, rw_ref, tok_part, og_part, tok_full, og_full, l_sem,
@@ -197,6 +197,11 @@
             device_id=where, device_id_type=MESH,
         )
 
+    near = list(range(n // 2 + 1))
+    distant = list(range(n // 2 + 1, n))
+    groups = (near, distant)
+    heights = [len(group) * slot for group in groups]
+    delta, turned = (delta_a, delta_b), (turned_a, turned_b)
     local = pltpu.make_async_copy
     loads = [
         local(tok_hbm.at[:, span(p, cols)], tok_part, l_sem.at[0]),
@@ -297,10 +302,10 @@
         )
 
     def act_from(j):
-        bit = 1
-        while bit < n and (j == 0 or bit < (j & -j)):
+        bit = (n if j == 0 else j & -j) // 2
+        while bit:
             act_copy(j + bit).start()
-            bit *= 2
+            bit //= 2
 
     def og_copy(i):
         return copy(og_send.at[i], og_all.at[core, i], o_s.at[i], o_r.at[i], {"ep": peer(i)})
@@ -315,8 +320,10 @@
         return copy(inner_tot, inner_ep.at[i], j_s.at[i], j_r.at[i], {"ep": peer(i)})
 
     def pair_copy(g, k):
+        at = pl.ds(0, heights[g])
         return copy(
-            pair_send.at[g, k], pair_recv.at[g, k], p_s.at[g, k], p_r.at[g, k], {"tp": buddy}
+            pair_send.at[g, k, at, :], pair_recv.at[g, k, at, :], p_s.at[g, k], p_r.at[g, k],
+            {"tp": buddy},
         )
 
     def far_copy(i):
@@ -334,16 +341,13 @@
     def snorm_copy(i):
         return copy(snorm_all.at[0], snorm_all.at[i], n_s.at[i], n_r.at[i], {"ep": peer(i)})
 
-    near = list(range(n // 2))
-    distant = list(range(n // 2, n))
-    groups = (near, distant)
-    height = n // 2 * slot
     tile = min(hid, 256)
 
     for i in range(1, n):
         dispatch(i).start()
     for load in own_loads:
         load.wait()
+    inner_tp[p] = jnp.zeros_like(inner_tp[p])
     if slot != cap:
         rows[:, 1:, cap:, :] = jnp.zeros((2, n - 1, slot - cap, width), BF16)
         back_recv[:, cap:, :] = jnp.zeros((n, slot - cap, cols), BF16)
@@ -367,8 +371,8 @@
     def forward(g, f):
         sources = slice(groups[g][0], groups[g][-1] + 1)
         at = slice(f * tile, (f + 1) * tile)
-        x_in = rows[0, sources].reshape(height, width)
-        x_cot = rows[1, sources].reshape(height, width)
+        x_in = rows[0, sources].reshape(heights[g], width)
+        x_cot = rows[1, sources].reshape(heights[g], width)
         gate_pre = lax.dot_general(wg[at, :], x_in, NT, preferred_element_type=F32)
         up_pre = lax.dot_general(wu[at, :], x_in, NT, preferred_element_type=F32)
         hidden_grad = lax.dot_general(wd[at, :], x_cot, NT, preferred_element_type=F32)
@@ -377,28 +381,33 @@
         hidden = (silu * up_pre).astype(BF16)
         up_d = (hidden_grad * silu).astype(BF16)
         gate_d = (hidden_grad * up_pre * sig * (1.0 + gate_pre * (1.0 - sig))).astype(BF16)
-        turned[g, 0, at, :] = gate_d
-        turned[g, 1, at, :] = up_d
-        turned[g, 2, at, :] = hidden
-        delta[g, 0, :, at] = gate_d.T
-        delta[g, 1, :, at] = up_d.T
+        turned[g][0, at, :] = gate_d
+        turned[g][1, at, :] = up_d
+        turned[g][2, at, :] = hidden
+        delta[g][0, :, at] = gate_d.T
+        delta[g][1, :, at] = up_d.T
         part_inner = jnp.sum(hidden.astype(F32) * hidden_grad, 0, keepdims=True)
-        inner_tp[p, g] = part_inner if f == 0 else inner_tp[p, g] + part_inner
+        if f:
+            part_inner = part_inner + inner_tp[p, g, :, 0 : heights[g]]
+        inner_tp[p, g, :, 0 : heights[g]] = part_inner
 
     def share(g, q):
         at = span(q, cols)
-        value = jnp.dot(delta[g, 0], wg[:, at], preferred_element_type=F32)
-        return value + jnp.dot(delta[g, 1], wu[:, at], preferred_element_type=F32)
-
-    def shares_far(g):
-        pair_send[g, 0] = share(g, mirror_buddy).astype(BF16)
+        value = jnp.dot(delta[g][0], wg[:, at], preferred_element_type=F32)
+        return value + jnp.dot(delta[g][1], wu[:, at], preferred_element_type=F32)
+
+    def shares_far(g, between=None):
+        own = pl.ds(0, heights[g])
+        pair_send[g, 0, own] = share(g, mirror_buddy).astype(BF16)
         pair_copy(g, 0).start()
-        acc_far[...] = share(g, mirror)
-        pair_send[g, 1] = share(g, buddy).astype(BF16)
+        acc_far[own] = share(g, mirror)
+        pair_send[g, 1, own] = share(g, buddy).astype(BF16)
         pair_copy(g, 1).start()
+        if between:
+            between()
         pair_copy(g, 0).wait_recv()
-        far = (acc_far[...] + pair_recv[g, 0].astype(F32)).astype(BF16)
-        far_send[groups[g][0] : groups[g][-1] + 1] = far.reshape(n // 2, slot, cols)
+        far = (acc_far[own] + pair_recv[g, 0, own].astype(F32)).astype(BF16)
+        far_send[groups[g][0] : groups[g][-1] + 1] = far.reshape(len(groups[g]), slot, cols)
 
     def far_start(g):
         for i in order[g]:
@@ -407,8 +416,8 @@
     def shares_own(g):
         value = share(g, p)
         pair_copy(g, 1).wait_recv()
-        value = value + pair_recv[g, 1].astype(F32)
-        acc_own[groups[g][0] : groups[g][-1] + 1] = value.reshape(n // 2, slot, cols)
+        value = value + pair_recv[g, 1, 0 : heights[g]].astype(F32)
+        acc_own[groups[g][0] : groups[g][-1] + 1] = value.reshape(len(groups[g]), slot, cols)
 
     def give_back(i):
         far_copy(i).wait_recv()
@@ -419,35 +428,36 @@
             back_send[i, 0:cap] = value
             back_copy(i).start()
 
-    order = (near[1:] + near[:1], distant)
+    order = (near[-1:] + near[1:-1], distant)
     steps = hid // tile
 
-    ahead = near[1:] + distant[:1]
-    for i in ahead:
+    for i in near[1:]:
         pass_on(i)
-    for i in near[1:]:
+    for i in near[1:-2]:
         from_mirror(i)
+    pass_on(distant[0])
+    from_mirror(near[-2])
+    from_mirror(near[-1])
+    for i in distant[1:-1]:
+        pass_on(i)
     for w in weights:
         w.wait()
     for i in near[1:]:
         settle(i)
-    rest = distant[1:]
-    tiles = [f for f in range(steps)]
-    for k, i in enumerate(rest):
-        pass_on(i)
-        if k == len(rest) - 1:
-            count = len(tiles)
-        else:
-            count = max(1, steps // (len(rest) - 1))
-        for f in tiles[:count]:
-            forward(0, f)
-        del tiles[:count]
-        from_mirror(distant[k])
+    for f in range(steps // 2):
+        forward(0, f)
+    pass_on(distant[-1])
     for load in late_loads:
         load.wait()
     act_from(0)
     for j in distant + near[1:]:
         og_copy(j).start()
+    for i in distant[:1]:
+        from_mirror(i)
+    for f in range(steps // 2, steps):
+        forward(0, f)
+    for i in distant[1:-1]:
+        from_mirror(i)
     shares_far(0)
     from_mirror(distant[-1])
     far_start(0)
@@ -459,8 +469,6 @@
         forward(1, f)
     for i in range(1, t):
         inner_copy(i).start()
-    shares_far(1)
-    far_start(1)
     levels = [1 << k for k in reversed(range(n.bit_length() - 1))]
 
     def act_level(low):
@@ -468,7 +476,6 @@
             act_copy(j).wait_recv()
             act_from(j)
 
-    act_level(levels[0])
     middle = [j for low in levels[1:-1] for j in range(low, n, 2 * low)]
 
     def act_next(count):
@@ -476,9 +483,16 @@
             act_copy(j).wait_recv()
             act_from(j)
         del middle[:count]
-
-    act_next(1)
-    for i in order[0]:
+    def meanwhile():
+        give_back(near[-1])
+        act_next(1)
+
+    act_level(levels[0])
+
+    shares_far(1, meanwhile)
+    far_start(1)
+    far_copy(0).start()
+    for i in near[1:-1]:
         give_back(i)
     shares_own(1)
 
@@ -492,11 +506,11 @@
         def step(c, carry):
             at = pl.ds(pl.multiple_of(c * block, block), block)
             value = jnp.dot(
-                turned[0, j], rows[source, 0 : n // 2, :, at].reshape(height, block),
+                turned_a[j], rows[source, : len(near), :, at].reshape(heights[0], block),
                 preferred_element_type=F32,
             )
             value = value + jnp.dot(
-                turned[1, j], rows[source, n // 2 :, :, at].reshape(height, block),
+                turned_b[j], rows[source, len(near) :, :, at].reshape(heights[1], block),
                 preferred_element_type=F32,
             )
             out[:, at] = value.astype(BF16)
@@ -526,36 +540,40 @@
     for k, i in enumerate(order[1]):
         spend(1)
         give_back(i)
-        if k:
-            act_next(1)
+        act_next(1)
     act_next(len(middle))
+    for i in range(1, n):
+        og_copy(i).wait_recv()
+    og_buddy().start()
+    spend(3)
+    og_buddy().wait_recv()
+    act_level(levels[-1])
+    shared = lax.dot_general(
+        act_all[...].reshape(n * toks, sh), og_all[...].reshape(n * toks, cut),
+        (((0,), (0,)), ((), ())), preferred_element_type=F32,
+    )
+    shared_out[...] = shared
+    snorm_all[0] = column_to_row(jnp.sum(shared * shared, 1, keepdims=True))
+    for i in range(1, n):
+        snorm_copy(i).start()
+    give_back(0)
     spend(len(todo))
     for j in range(3):
         norms_out[j] = column_to_row(jnp.sum(squares[j], 1, keepdims=True))
     for i in range(1, n):
-        og_copy(i).wait_recv()
-    og_buddy().start()
-    act_level(levels[-1])
-    og_buddy().wait_recv()
-    shared = lax.dot_general(
-        act_all[...].reshape(n * toks, sh), og_all[...].reshape(n * toks, cut),
-        (((0,), (0,)), ((), ())), preferred_element_type=F32,
-    )
-    shared_out[...] = shared
-    snorm_all[0] = column_to_row(jnp.sum(shared * shared, 1, keepdims=True))
-    for i in range(1, n):
-        snorm_copy(i).start()
-    for i in range(1, n):
         inner_back(i).wait_recv()
     found = jnp.zeros((n, toks), F32)
     for g in range(2):
-        block_of = lax.broadcasted_iota(jnp.int32, (n, height), 1) // slot + g * n // 2
-        row_of = lax.broadcasted_iota(jnp.int32, (n, height), 0)
-        spread = jnp.zeros((n, height), F32)
+        low, size = groups[g][0] * slot, heights[g]
+        block_of = lax.broadcasted_iota(jnp.int32, (n, size), 1) // slot + groups[g][0]
+        row_of = lax.broadcasted_iota(jnp.int32, (n, size), 0)
+        spread = jnp.zeros((n, size), F32)
         for i in groups[g]:
-            spread = jnp.where((block_of == i) & (row_of == i), inner_ep[i, g], spread)
+            spread = jnp.where(
+                (block_of == i) & (row_of == i), inner_ep[i, g, :, 0:size], spread
+            )
         found = found + jnp.dot(
-            spread, picks[g * height : (g + 1) * height, :].astype(F32),
+            spread, picks[low : low + size, :].astype(F32),
             precision=lax.Precision.HIGHEST, preferred_element_type=F32,
         )
     for k in range(2):
@@ -618,7 +636,7 @@
     cut = width // n
     part = toks // 2
     total = n * slot
-    height = total // 2
+    high, low = (n // 2 + 1) * slot, (n // 2 - 1) * slot
     vmem = pl.BlockSpec(memory_space=pltpu.VMEM)
     hbm = pl.BlockSpec(memory_space=pl.ANY)
     dma = pltpu.SemaphoreType.DMA
@@ -645,20 +663,22 @@
             pltpu.VMEM((total, toks), BF16),
             pltpu.VMEM((128, toks), F32),
             pltpu.VMEM((128, toks), F32),
-            pltpu.VMEM((2, 2, height, hid), BF16),
-            pltpu.VMEM((2, 3, hid, height), BF16),
+            pltpu.VMEM((2, high, hid), BF16),
+            pltpu.VMEM((2, low, hid), BF16),
+            pltpu.VMEM((3, hid, high), BF16),
+            pltpu.VMEM((3, hid, low), BF16),
             pltpu.VMEM((3, hid, 128), F32),
-            pltpu.VMEM((2, 2, height, cols), BF16),
-            pltpu.VMEM((2, 2, height, cols), BF16),
-            pltpu.VMEM((height, cols), F32),
+            pltpu.VMEM((2, 2, high, cols), BF16),
+            pltpu.VMEM((2, 2, high, cols), BF16),
+            pltpu.VMEM((high, cols), F32),
             pltpu.VMEM((n, slot, cols), F32),
             pltpu.VMEM((n, slot, cols), BF16),
             pltpu.VMEM((n, slot, cols), BF16),
             pltpu.VMEM((n, slot, cols), BF16),
             pltpu.VMEM((n, slot, cols), BF16),
-            pltpu.VMEM((t, 2, 1, height), F32),
-            pltpu.VMEM((2, 1, height), F32),
-            pltpu.VMEM((n, 2, 1, height), F32),
+            pltpu.VMEM((t, 2, 1, high), F32),
+            pltpu.VMEM((2, 1, high), F32),
+            pltpu.VMEM((n, 2, 1, high), F32),
             pltpu.VMEM((2, n, part, sh), BF16),
             pltpu.VMEM((n, part, cut), BF16),
             pltpu.VMEM((2, n, part, cut), BF16),

time: 51.3 us -> 48.4 us (0.943)
  Pallas kernels: 50.5 us -> 47.6 us
    pallas_call x1, Pallas kernels: 47.5 us -> 44.7 us  [fused(): pl.pallas_call(functools.partial(kernel, n, t, cap, slot), out_shape=(plt...]
where the time goes in v3:
time: 48.4 us; the launch traced here: 48.2 us
  Pallas kernels  47.6 us (98%)
  between operations  0.64 us (1%)
    pallas_call x1, Pallas kernels, fused(): pl.pallas_call(functools.partial(kernel, n, t, cap, slot), out_shape=(plt...  44.7 us
    pallas_call x1, Pallas kernels, fused(): pl.pallas_call(hand_over, out_shape=[jax.ShapeDtypeStruct(r.shape, r.dtyp...  2.91 us

profile of v3, /device:TPU:0, one launch (start us, length us, event | category | flops | bytes accessed | tf_op | source)
XLA Modules:
  0.0 48.2 jit_solution(432507563408053817)
XLA Ops:
  0.6 44.7 %shard_map.143 = (bf16[128,512]{1,0:T(8,128)(2,1)S(1)}, f32[2,128]{1,0:T(2,128)S(1)}, bf16[512,2048]{1,0:T(8,128)(2,1)S(1)}, bf16[512,2048]{1,0:T(8,128)(2,1)S(1...) custom-call(s32[2,128]{1,0:T(2,128)} %bitcast.8, ...), custom_call_target="tpu_custom_call" | custom-call | tf_op jit(solution)/shard_map/pallas_call | solution.py:643
  45.3 2.9 %shard_map.144 = (bf16[128,512]{1,0:T(8,128)(2,1)}, f32[2,128]{1,0:T(2,128)}, bf16[512,2048]{1,0:T(8,128)(2,1)}, bf16[512,2048]{1,0:T(8,128)(2,1)}, bf16[512,204...) custom-call(bf16[128,512]{1,0:T(8,128)(2,1)S(1)} %get-tuple-element.24.refs_0_, ...), custom_call_target="tpu_custom_call" | custom-call | tf_op jit(solution)/shard_map/pallas_call | solution.py:712
